TPU v7x, 32 devices: a whole 2x2x4 slice. The times are simulated.
32 devices in a mesh: ep: 8 (over z, y), tp: 4 (over x, core).
Axes of the slice: x: 2, y: 2, z: 4, core: 2. Of those that a mesh axis runs over, the one named last changes fastest.
Arguments:
- mixer_input: bfloat16 [4096, 2048], P(('ep', 'tp')), may hold values from -6 to 6
- expert_input: bfloat16 [4096, 2048], P(('ep', 'tp')), may hold values from -6 to 6
- mixer_gain: float32 [2048], replicated, may hold values from 0.1 to 1.9
- expert_gain: float32 [2048], replicated, may hold values from 0.1 to 1.9
- query_weight: bfloat16 [2048, 1024], P(None, 'tp'), may hold values from -0.125 to 0.125
- key_weight: bfloat16 [2048, 1024], P(None, 'tp'), may hold values from -0.125 to 0.125
- value_weight: bfloat16 [2048, 1024], P(None, 'tp'), may hold values from -0.125 to 0.125
- out_weight: bfloat16 [1024, 2048], P('tp'), may hold values from -0.1875 to 0.1875
- decay_rate: float32 [8], P('tp'), may hold values from 0 to 0.12
- routing: int32 [4096, 4], P('ep'), may hold values from 0 to 7, all different within a row; in each aligned block of 128 rows (0 to 127, 128 to 255, ...) at most 96 rows name the same one
- route_weight: float32 [4096, 4], P('ep'), may hold values from 0.2 to 1
- gate_weight: bfloat16 [8, 2048, 1024], P('ep', None, 'tp'), may hold values from -0.125 to 0.125
- up_weight: bfloat16 [8, 2048, 1024], P('ep', None, 'tp'), may hold values from -0.125 to 0.125
- down_weight: bfloat16 [8, 1024, 2048], P('ep', None, 'tp'), may hold values from -0.1875 to 0.1875
- shared_gate: bfloat16 [2048, 512], P(None, 'tp'), may hold values from -0.125 to 0.125
- shared_up: bfloat16 [2048, 512], P(None, 'tp'), may hold values from -0.125 to 0.125
- shared_down: bfloat16 [512, 2048], P(None, 'tp'), may hold values from -0.25 to 0.25
Outputs:
- mixer_output: float32 [4096, 2048], P(('ep', 'tp'))
- expert_output: float32 [4096, 2048], P('ep', 'tp')
Inputs may be any that keep to these rules, and one draw needn't show every extreme that they name: `routing`: each row names 4 different experts. In each aligned block of 128 rows, no expert is named by more than 96 rows, and in some blocks one expert is named by exactly 96 rows.
All inputs are finite; a program needn't handle non-finite values.
Results may differ from a plain program's by a relative error of at most 0.0095.
Values may be sent and summed in bfloat16 or wider, within the bound.
A program may use at most 128 MiB of HBM per device.

v0:
```python
import jax
import jax.numpy as jnp
from jax import lax
from jax.sharding import PartitionSpec as P

HD = 128
BLK = 64


NORM_EPS = 1e-06
ROPE_BASE = 10000.0
EXACT_MATMUL = lax.Precision.HIGHEST


def prefix(part, axis, combine, identity):
    place = lax.axis_index(axis)
    gathered = jax.tree.map(lambda a: lax.all_gather(a, axis), part)
    state = jax.tree.map(lambda a, e: jnp.zeros_like(a) + jnp.asarray(e, a.dtype), part, identity)

    def one(turn, state):
        return combine(
            state, jax.tree.map(lambda a: lax.dynamic_index_in_dim(a, turn, 0, False), gathered)
        )

    return lax.fori_loop(0, place, one, state)


def norm_rows(inputs, gain_vector):
    values = inputs.astype(jnp.float32)
    scaled = values * lax.rsqrt(jnp.mean(values * values, axis=-1, keepdims=True) + NORM_EPS)
    return (scaled * gain_vector).astype(jnp.bfloat16)


def rotate(head_rows, positions):
    head_size = head_rows.shape[-1]
    inverse = ROPE_BASE ** (-jnp.arange(0, head_size, 2, dtype=jnp.float32) / head_size)
    angles = positions[:, None] * inverse[None, :]
    cosine = jnp.cos(angles)[:, None, :]
    sine_part = jnp.sin(angles)[:, None, :]
    front_half = head_rows[..., : head_size // 2]
    behind = head_rows[..., head_size // 2 :]
    return jnp.concatenate(
        [front_half * cosine - behind * sine_part, front_half * sine_part + behind * cosine],
        axis=-1,
    )


def project(inputs, weight, head_total):
    product = jnp.dot(inputs, weight, preferred_element_type=jnp.float32).astype(jnp.bfloat16)
    product = lax.optimization_barrier(product)
    return product.astype(jnp.float32).reshape(inputs.shape[0], head_total, -1)


def chain_combine(earlier, latter):
    return (earlier[0] * latter[0], latter[0][:, None, None] * earlier[1] + latter[1])


def retain_local(query_heads, key_heads, value_heads, decay_rates):
    length, head_total, head_size = query_heads.shape
    blocks = length // BLK
    log_gamma = -decay_rates
    inner_pos = jnp.arange(BLK, dtype=jnp.float32)
    offsets = inner_pos[:, None] - inner_pos[None, :]
    inside_block_output = jnp.where(
        offsets >= 0, jnp.exp(log_gamma[:, None, None] * jnp.maximum(offsets, 0.0)), 0.0
    )
    key_scale = jnp.exp(log_gamma[None, :] * (BLK - 1.0 - inner_pos)[:, None])
    query_scale = jnp.exp(log_gamma[None, :] * (inner_pos + 1.0)[:, None])
    blocked = (blocks, BLK, head_total, head_size)
    q_blocks = query_heads.reshape(blocked)
    k_blocks = key_heads.reshape(blocked)
    v_blocks = value_heads.reshape(blocked)
    attention_scores = (
        jnp.einsum("nchd,nmhd->nhcm", q_blocks, k_blocks, precision=EXACT_MATMUL)
        * inside_block_output[None]
    )
    nearby = jnp.einsum("nhcm,nmhe->nche", attention_scores, v_blocks, precision=EXACT_MATMUL)
    block_states = jnp.einsum(
        "nchd,nche->nhde", k_blocks * key_scale[None, :, :, None], v_blocks, precision=EXACT_MATMUL
    )
    block_offset_rows = jnp.arange(blocks, dtype=jnp.float32)
    to_end = jnp.exp(log_gamma[None, :] * BLK * (blocks - 1.0 - block_offset_rows)[:, None])
    summary = jnp.einsum("nh,nhde->hde", to_end, block_states, precision=EXACT_MATMUL)
    through = jnp.exp(log_gamma * (BLK * blocks))
    incoming = prefix(
        (through, summary), "ep", chain_combine, (jnp.ones_like(through), jnp.zeros_like(summary))
    )[1]
    block_gaps = block_offset_rows[:, None] - 1.0 - block_offset_rows[None, :]
    carry_mix = jnp.where(
        block_gaps >= 0, jnp.exp(log_gamma[:, None, None] * BLK * jnp.maximum(block_gaps, 0.0)), 0.0
    )
    entering = jnp.einsum("hbj,jhde->bhde", carry_mix, block_states, precision=EXACT_MATMUL)
    entering = (
        entering
        + jnp.exp(log_gamma[None, :] * BLK * block_offset_rows[:, None])[:, :, None, None]
        * incoming[None]
    )
    distant = jnp.einsum(
        "bchd,bhde->bche",
        q_blocks * query_scale[None, :, :, None],
        entering,
        precision=EXACT_MATMUL,
    )
    retained = (nearby + distant).reshape(length, head_total, head_size)
    normed = retained * lax.rsqrt(jnp.mean(retained * retained, axis=-1, keepdims=True) + NORM_EPS)
    return normed.astype(jnp.bfloat16).reshape(length, head_total * head_size)


def assign_slots(routes, source_rows, capacity, expert_count):
    token_count, pick_count = routes.shape
    chosen = routes.reshape(token_count * pick_count)
    onehot = (chosen[:, None] == jnp.arange(expert_count, dtype=jnp.int32)[None, :]).astype(
        jnp.int32
    )
    per_source = onehot.reshape(token_count // source_rows, source_rows * pick_count, expert_count)
    earlier_hits = jnp.cumsum(per_source, axis=1) - per_source
    ranks = jnp.sum(earlier_hits * per_source, axis=2).reshape(token_count * pick_count)
    sources = jnp.arange(token_count * pick_count, dtype=jnp.int32) // (source_rows * pick_count)
    return (chosen, sources * capacity + ranks)


def gather_slots(token_rows, chosen, slot_ids, slot_count, expert_count, pick_count):
    owners = jnp.arange(chosen.shape[0], dtype=jnp.int32) // pick_count + 1
    owner_table = jnp.zeros((slot_count, expert_count), jnp.int32).at[slot_ids, chosen].set(owners)
    padded = jnp.concatenate(
        [jnp.zeros((1, token_rows.shape[1]), token_rows.dtype), token_rows], axis=0
    )
    return padded[owner_table]


def expert_hidden(routed_rows, gate_weight, up_weight):
    per_device = gate_weight.shape[0]
    grouped = routed_rows.reshape(
        routed_rows.shape[0], routed_rows.shape[1] // per_device, per_device, routed_rows.shape[2]
    )
    gate_part = jnp.einsum(
        "snxd,xdf->snxf", grouped, gate_weight, preferred_element_type=jnp.float32
    )
    up_part = jnp.einsum("snxd,xdf->snxf", grouped, up_weight, preferred_element_type=jnp.float32)
    return (jax.nn.silu(gate_part) * up_part).astype(jnp.bfloat16)


def shards(
    mixer_input,
    expert_input,
    mixer_gain,
    expert_gain,
    query_weight,
    key_weight,
    value_weight,
    out_weight,
    decay_rate,
    routing,
    route_weight,
    gate_weight,
    up_weight,
    down_weight,
    shared_gate,
    shared_up,
    shared_down,
):
    own_count = mixer_input.shape[0]
    tp_index = lax.axis_index("tp")
    own_expert_rows = norm_rows(expert_input, expert_gain)
    mixer_rows, expert_rows = (
        lax.all_gather(norm_rows(mixer_input, mixer_gain), "tp", axis=0, tiled=True),
        lax.all_gather(own_expert_rows, "tp", axis=0, tiled=True),
    )
    group_count = mixer_rows.shape[0]
    head_total = decay_rate.shape[0]
    positions = (
        lax.axis_index("ep") * group_count + jnp.arange(group_count, dtype=jnp.int32)
    ).astype(jnp.float32)
    query_heads = rotate(project(mixer_rows, query_weight, head_total), positions) * HD ** (-0.5)
    key_heads = rotate(project(mixer_rows, key_weight, head_total), positions)
    value_heads = project(mixer_rows, value_weight, head_total)
    mixed_heads = retain_local(query_heads, key_heads, value_heads, decay_rate)
    mixer_output = lax.psum_scatter(
        jnp.dot(mixed_heads, out_weight, preferred_element_type=jnp.float32).astype(jnp.bfloat16),
        "tp",
        scatter_dimension=0,
        tiled=True,
    ).astype(jnp.float32)
    expert_count = lax.axis_size("ep") * gate_weight.shape[0]
    pick_count = routing.shape[1]
    capacity = (3 * own_count * pick_count + 2 * expert_count - 1) // (2 * expert_count)
    chosen, slot_ids = assign_slots(routing, own_count, capacity, expert_count)
    own_span = own_count * pick_count
    own_chosen = lax.dynamic_slice_in_dim(chosen, tp_index * own_span, own_span, 0)
    own_slots = (
        lax.dynamic_slice_in_dim(slot_ids, tp_index * own_span, own_span, 0) - tp_index * capacity
    )
    outgoing = gather_slots(
        own_expert_rows, own_chosen, own_slots, capacity, expert_count, pick_count
    )
    arrived = lax.all_to_all(outgoing, "ep", split_axis=1, concat_axis=1, tiled=True)
    hidden = expert_hidden(
        lax.all_gather(arrived, "tp", axis=0, tiled=True), gate_weight, up_weight
    )
    shared_hidden = (
        jax.nn.silu(jnp.dot(expert_rows, shared_gate, preferred_element_type=jnp.float32))
        * jnp.dot(expert_rows, shared_up, preferred_element_type=jnp.float32)
    ).astype(jnp.bfloat16)
    full_hidden, full_shared = (
        lax.all_gather(hidden, "tp", axis=3, tiled=True),
        lax.all_gather(shared_hidden, "tp", axis=1, tiled=True),
    )
    results = jnp.einsum(
        "snxf,xfe->snxe", full_hidden, down_weight, preferred_element_type=jnp.float32
    ).astype(jnp.bfloat16)
    results = results.reshape(results.shape[0], expert_count, results.shape[3])
    returned = lax.all_to_all(results, "ep", split_axis=1, concat_axis=1, tiled=True)
    flat_results = returned.reshape(returned.shape[0] * expert_count, returned.shape[2])
    picked = flat_results[slot_ids * expert_count + chosen].astype(jnp.float32)
    weighted = jnp.sum(
        picked.reshape(group_count, pick_count, -1) * route_weight[:, :, None], axis=1
    )
    shared_result = jnp.dot(full_shared, shared_down, preferred_element_type=jnp.float32)
    expert_output = weighted + shared_result
    return (mixer_output, expert_output)


def solution(mesh):
    return jax.shard_map(
        shards,
        mesh=mesh,
        in_specs=(
            P(("ep", "tp"), None),
            P(("ep", "tp"), None),
            P(),
            P(),
            P(None, "tp"),
            P(None, "tp"),
            P(None, "tp"),
            P("tp", None),
            P("tp"),
            P("ep", None),
            P("ep", None),
            P("ep", None, "tp"),
            P("ep", None, "tp"),
            P("ep", None, "tp"),
            P(None, "tp"),
            P(None, "tp"),
            P(None, "tp"),
        ),
        out_specs=(P(("ep", "tp"), None), P("ep", "tp")),
        check_vma=False,
    )
```

profile of v0, /device:TPU:0, one launch (start us, length us, event | category | flops | bytes accessed | tf_op | source)
XLA Modules:
  0.0 451.2 jit_solution(2308968896453335702)
XLA Ops:
  9.9 4.5 %reduce-window.6 = s32[4,8,4,128]{3,1,2,0:T(8,128)S(1)} reduce-window(s32[4,8,4,128]{3,1,2,0:T(8,128)S(1)} %fusion.42, s32[]{:T(128)} %constant.109.clone.1), window={size=1x1x1x128 pad=0_0x0_0x0_0x127_0}, to_apply=%region_6.7 | reduce-window | flops 2080768 | bytes 131076 | tf_op jit(solution)/shard_map/reduce-window
  15.2 22.0 %scatter_fusion = s32[96,8]{0,1:T(8,128)S(1)} fusion(s32[96,8]{0,1:T(8,128)S(1)} %broadcast.366, s32[512]{0:T(512)S(1)} %bitcast.124, s32[512]{0:T(512)S(1)} %fusion.65), kind=kCustom, calls=%fused_computation.2 | custom fusion | bytes 10240 | tf_op jit(solution)/shard_map/scatter | solution.py:124
  37.7 4.2 gather_fusion
  42.0 3.6 copy.110
  45.6 77.9 %all_to_all.10 = bf16[96,8,2048]{2,0,1:T(8,128)(2,1)} all-to-all(bf16[96,8,2048]{2,0,1:T(8,128)(2,1)S(1)} %copy.110), channel_id=1, replica_groups=mesh['ep'=8,'tp'=4] {'ep'}, dimensions={1} | all-to-all | bytes 6291456 | tf_op jit(solution)/shard_map/all_to_all | solution.py:196
  125.8 79.0 %all-gather.10.cloned.1.call-done = bf16[384,8,2048]{2,0,1:T(8,128)(2,1)} async-done(((bf16[96,8,2048]{2,0,1:T(8,128)(2,1)}), bf16[384,8,2048]{2,0,1:T(8,128)(2,1)}) %all-gather.10.cloned.1.call-update) | async-done | bytes 12582928 | tf_op jit(solution)/shard_map/all_gather | solution.py:198
  204.8 6.7 %fusion.19 = f32[384,8,256]{2,0,1:T(8,128)S(1)} fusion(bf16[384,8,2048]{2,0,1:T(8,128)(2,1)} %all-gather.10.cloned.1.call-done, bf16[1,2048,256]{2,1,0:T(8,128)(2,1)S(1)} %copy-done.14), kind=kOutput, calls=%fused_computation.40 | convolution fusion | flops 3221225472 | bytes 16777216 | tf_op jit(solution)/shard_map/snxd,xdf->snxf/dot_general | solution.py:139
  213.0 6.4 %fusion.2 = bf16[384,8,1,256]{3,0,1,2:T(8,128)(2,1)} fusion(f32[384,8,256]{2,0,1:T(8,128)S(1)} %fusion.19, bf16[384,8,2048]{2,0,1:T(8,128)(2,1)S(1)} %copy-done.13, bf16[1,2048,256]{2,1,0:T(8,128)(2,1)} %param.30), kind=kOutput, calls=%fused_computation.9 | convolution fusion | flops 3225944064 | bytes 18350080 | tf_op jit(solution)/shard_map/snxd,xdf->snxf/dot_general | solution.py:136
  223.4 6.2 %all-gather.8.cloned.1.call-done = bf16[512,2048]{1,0:T(8,128)(2,1)} async-done(((bf16[128,2048]{1,0:T(8,128)(2,1)}), bf16[512,2048]{1,0:T(8,128)(2,1)}) %all-gather.8.cloned.1.call-update) | async-done | bytes 2097168 | tf_op jit(solution)/shard_map/all_gather | solution.py:166
  229.5 2.6 convolution_convert_fusion.1
  232.4 2.6 convolution_convert_fusion.3
  235.7 2.8 convolution_convert_fusion.2
  242.3 2.1 fusion.23
  245.8 21.2 %all-reduce.1 = f32[16]{0:T(128)S(1)} all-reduce(f32[16]{0:T(128)S(1)} %get-tuple-element.74), channel_id=2, replica_groups=mesh['ep'=8,'tp'=4] {'ep'}, use_global_device_ids=true, to_apply=%add.1 | all-reduce | flops 16 | bytes 128
  269.9 2.1 fusion.38
  272.0 6.3 %all-gather.12.cloned.1.call-done = bf16[384,8,1,1024]{3,0,1,2:T(8,128)(2,1)} async-done(((bf16[384,8,1,256]{3,0,1,2:T(8,128)(2,1)}), bf16[384,8,1,1024]{3,0,1,2:T(8,128)(2,1)}) %all-gather.12.cloned.1.call-update) | async-done | bytes 6291472 | tf_op jit(solution)/shard_map/all_gather | solution.py:205
  278.3 7.6 %fusion.6 = bf16[384,8,512]{2,0,1:T(8,128)(2,1)} fusion(bf16[384,8,1,1024]{3,0,1,2:T(8,128)(2,1)} %all-gather.12.cloned.1.call-done, bf16[1,1024,512]{2,1,0:T(8,128)(2,1)S(1)} %copy-done), kind=kOutput, calls=%fused_computation.17 | convolution fusion | flops 3222798336 | bytes 10485760 | tf_op jit(solution)/shard_map/snxf,xfe->snxe/dot_general | solution.py:208
  285.9 5.5 %all-to-all-start.1 = ((bf16[384,8,512]{2,0,1:T(8,128)(2,1)}), bf16[384,8,512]{2,0,1:T(8,128)(2,1)}, u32[]{:S(2)}, u32[]{:S(2)}) async-start(bf16[384,8,512]{2,0,1:T(8,128)(2,1)} %fusion.6), calls=%async_computation.2 | async-start | bytes 6291456 | tf_op jit(solution)/shard_map/all_to_all | solution.py:212
  291.5 70.6 %all-gather.16.cloned.1.call-done = f32[16,128,128]{2,1,0:T(8,128)} async-done(((f32[2,128,128]{2,1,0:T(8,128)}), f32[16,128,128]{2,1,0:T(8,128)}) %all-gather.16.cloned.1.call-update) | async-done | bytes 1048592 | tf_op jit(solution)/shard_map/all_gather | solution.py:17
  362.4 2.3 fusion.9
  364.7 2.3 multiply_reduce_fusion.1
  368.2 3.4 convolution_convert_fusion
  372.1 12.0 %all-gather.14.cloned.1.call-done = bf16[512,2048]{1,0:T(8,128)(2,1)} async-done(((bf16[128,2048]{1,0:T(8,128)(2,1)}), bf16[512,2048]{1,0:T(8,128)(2,1)}) %all-gather.14.cloned.1.call-update) | async-done | bytes 2097168 | tf_op jit(solution)/shard_map/all_gather | solution.py:167
  384.1 2.3 fusion.79
  386.4 2.3 fusion.11
  388.8 7.7 %all_gather.35 = bf16[512,512]{1,0:T(8,128)(2,1)} all-gather(bf16[512,128]{1,0:T(8,128)(2,1)S(1)} %fusion.11), channel_id=1, replica_groups=mesh['ep'=8,'tp'=4] {'tp'}, dimensions={1}, use_global_device_ids=true | all-gather | bytes 655360 | tf_op jit(solution)/shard_map/all_gather | solution.py:206
  396.4 21.3 %reduce-scatter.2.cloned.1.call-done = bf16[128,2048]{1,0:T(8,128)(2,1)} async-done(((bf16[512,2048]{1,0:T(8,128)(2,1)}), bf16[128,2048]{1,0:T(8,128)(2,1)}) %reduce-scatter.2.cloned.1.call-update) | async-done | bytes 524304 | tf_op jit(solution)/shard_map/reduce_scatter | solution.py:178
  417.7 2.1 convert_element_type.76
  419.8 5.3 %copy.175 = bf16[384,8,512]{2,1,0:T(8,128)(2,1)} copy(bf16[384,8,512]{2,0,1:T(8,128)(2,1)} %all-to-all-done.1) | data formatting | bytes 6291456 | tf_op jit(solution)/shard_map/all_to_all | solution.py:212
  425.2 9.9 %gather_fusion.1 = bf16[2048,512]{1,0:T(8,128)(2,1)S(1)} fusion(bf16[3072,512]{1,0:T(8,128)(2,1)} %bitcast.123, s32[2048]{0:T(1024)S(1)} %broadcast_clamp_fusion), kind=kCustom, calls=%fused_computation.1 | custom fusion | bytes 4202496 | tf_op jit(solution)/shard_map/gather | solution.py:214
  435.1 3.0 reshape.411
  438.1 4.9 %multiply_reduce_fusion = f32[512,512]{1,0:T(8,128)S(1)} fusion(f32[512,4,512]{2,1,0:T(4,128)} %reshape.411, f32[512,4]{1,0:T(8,128)S(1)} %copy.113), kind=kLoop, calls=%fused_computation.7 | loop fusion | flops 1835008 | bytes 5251072 | tf_op jit(solution)/shard_map/reduce_sum | solution.py:215
  (109 shorter events, 23.0 us)
Async XLA Ops:
  7.2 271.2 %copy-start = (bf16[1,1024,512]{2,1,0:T(8,128)(2,1)S(1)}, bf16[1,1024,512]{2,1,0:T(8,128)(2,1)}, u32[]{:S(2)}) copy-start(bf16[1,1024,512]{2,1,0:T(8,128)(2,1)} %param.32) | copy-start | bytes 3145732
  7.2 197.6 %all-gather.10.cloned.1.call-start = ((), (), s32[]{:S(2)}) async-start(), calls=%async_computation.5 | async-start | bytes 15728640 | tf_op jit(solution)/shard_map/all_gather | solution.py:198
  8.2 29.2 %copy-start.4 = (bf16[128,2048]{1,0:T(8,128)(2,1)S(1)}, bf16[128,2048]{1,0:T(8,128)(2,1)}, u32[]{:S(2)}) copy-start(bf16[128,2048]{1,0:T(8,128)(2,1)} %param.20) | copy-start | bytes 1572868
  8.2 29.2 %copy-start.9 = (f32[2048]{0:T(1024)S(1)}, f32[2048]{0:T(1024)}, u32[]{:S(2)}) copy-start(f32[2048]{0:T(1024)} %param.22) | copy-start | bytes 24580
  37.6 4.4 copy-start.1
  123.5 1.0 copy-start.5
  123.5 1.2 copy-start.10
  123.5 81.3 %copy-start.14 = (bf16[1,2048,256]{2,1,0:T(8,128)(2,1)S(1)}, bf16[1,2048,256]{2,1,0:T(8,128)(2,1)}, u32[]{:S(2)}) copy-start(bf16[1,2048,256]{2,1,0:T(8,128)(2,1)} %param.31) | copy-start | bytes 3145732
  123.6 106.0 %all-gather.8.cloned.1.call-start = ((), (), s32[]{:S(2)}) async-start(), calls=%async_computation.3 | async-start | bytes 2621440 | tf_op jit(solution)/shard_map/all_gather | solution.py:166
  125.8 152.5 %all-gather.12.cloned.1.call-start = ((), (), s32[]{:S(2)}) async-start(), calls=%async_computation.6 | async-start | bytes 7864320 | tf_op jit(solution)/shard_map/all_gather | solution.py:205
  204.8 8.2 %copy-start.13 = (bf16[384,8,2048]{2,0,1:T(8,128)(2,1)S(1)}, bf16[384,8,2048]{2,0,1:T(8,128)(2,1)}, u32[]{:S(2)}) copy-start(bf16[384,8,2048]{2,0,1:T(8,128)(2,1)} %all-gather.10.cloned.1.call-done) | copy-start | bytes 37748740
  213.0 6.5 %copy-start.16 = (u32[32]{0:T(128)S(1)}, u32[32]{0:T(128)}, u32[]{:S(2)}) copy-start(u32[32]{0:T(128)} %constant.150) | copy-start | bytes 388
  213.0 7.8 %copy-start.12 = (f32[2]{0:T(128)S(1)}, f32[2]{0:T(128)}, u32[]{:S(2)}) copy-start(f32[2]{0:T(128)} %param.27) | copy-start | bytes 28
  219.5 142.6 %all-gather.16.cloned.1.call-start = ((), (), s32[]{:S(2)}) async-start(), calls=%async_computation.8 | async-start | bytes 1179648 | tf_op jit(solution)/shard_map/all_gather | solution.py:17
  240.0 1.3 copy-start.3
  244.5 139.7 %all-gather.14.cloned.1.call-start = ((), (), s32[]{:S(2)}) async-start(), calls=%async_computation.7 | async-start | bytes 2621440 | tf_op jit(solution)/shard_map/all_gather | solution.py:167
  285.9 133.9 %all-to-all-start.1 = ((bf16[384,8,512]{2,0,1:T(8,128)(2,1)}), bf16[384,8,512]{2,0,1:T(8,128)(2,1)}, u32[]{:S(2)}, u32[]{:S(2)}) async-start(bf16[384,8,512]{2,0,1:T(8,128)(2,1)} %fusion.6), calls=%async_computation.2 | async-start | bytes 6291456 | tf_op jit(solution)/shard_map/all_to_all | solution.py:212
  291.4 73.2 %copy-start.2 = (f32[512,2,64]{2,0,1:T(8,128)S(1)}, f32[512,2,64]{2,0,1:T(8,128)}, u32[]{:S(2)}) copy-start(f32[512,2,64]{2,0,1:T(8,128)} %get-tuple-element.58) | copy-start | bytes 786436
  291.4 126.3 %reduce-scatter.2.cloned.1.call-start = ((), (), s32[]{:S(2)}) async-start(), calls=%async_computation.4 | async-start | bytes 2621440 | tf_op jit(solution)/shard_map/reduce_scatter | solution.py:178
  368.2 3.7 copy-start.11
  368.2 15.9 %copy-start.7 = (bf16[2048,128]{1,0:T(8,128)(2,1)S(1)}, bf16[2048,128]{1,0:T(8,128)(2,1)}, u32[]{:S(2)}) copy-start(bf16[2048,128]{1,0:T(8,128)(2,1)} %param.33) | copy-start | bytes 1572868
  371.7 14.8 %copy-start.15 = (bf16[2048,128]{1,0:T(8,128)(2,1)S(1)}, bf16[2048,128]{1,0:T(8,128)(2,1)}, u32[]{:S(2)}) copy-start(bf16[2048,128]{1,0:T(8,128)(2,1)} %param.34) | copy-start | bytes 1572868
  438.1 4.9 %copy-start.6 = (bf16[512,512]{1,0:T(8,128)(2,1)S(1)}, bf16[512,512]{1,0:T(8,128)(2,1)}, u32[]{:S(2)}) copy-start(bf16[512,512]{1,0:T(8,128)(2,1)} %all_gather.35) | copy-start | bytes 1572868
  438.1 4.9 %copy-start.8 = (bf16[512,512]{1,0:T(8,128)(2,1)S(1)}, bf16[512,512]{1,0:T(8,128)(2,1)}, u32[]{:S(2)}) copy-start(bf16[512,512]{1,0:T(8,128)(2,1)} %param.35) | copy-start | bytes 1572868
Sparse Core Ops, SparseCore 0:
  123.7 81.0 all-gather.9
  206.9 22.5 all-gather.7
  231.1 47.1 all-gather.11
  280.3 81.7 all-gather.15
  363.5 20.5 all-gather.13
  386.5 31.1 reduce-scatter.1
where the time goes:
time: 452 us; the launch traced here: 451 us
  waiting for transfers between devices  196 us (43%)
  blocking collectives  107 us (24%)
  local copies, waits for them, and re-layouts  57.9 us (13%)
  matrix products  50.2 us (11%)
  other arithmetic  19 us (4%)
  between operations  15.3 us (3%)
  starting transfers between devices  5.76 us (1%)
    all_gather x1, waiting for transfers between devices, shards(): lax.all_gather(arrived, 'tp', axis=0, tiled=True)  79 us
    all_to_all x1, blocking collectives, shards(): lax.all_to_all(outgoing, 'ep', split_axis=1, concat_axis=1, tiled=True)  77.9 us
    all_gather x1, waiting for transfers between devices, prefix(): gathered = jax.tree.map(lambda a: lax.all_gather(a, axis), part)  70.6 us
    scatter x1, local copies, waits for them, and re-layouts, gather_slots(): jnp.zeros((slot_count, expert_count), jnp.int32).at[slot_ids, chosen]  22 us
    reduce_scatter x1, waiting for transfers between devices, shards(): lax.psum_scatter(jnp.dot(mixed_heads, out_weight, preferred_element_type=...  21.3 us
    unnamed x1, blocking collectives  21.2 us
    all_gather x1, waiting for transfers between devices, shards(): lax.all_gather(own_expert_rows, 'tp', axis=0, tiled=True)  12 us
    gather x1, local copies, waits for them, and re-layouts, shards(): picked = flat_results[slot_ids * expert_count + chosen].astype(jnp.float32)  9.88 us
  transfers between devices with their start and end apart: 7, of which 6 were waited for; matrix products, arithmetic and copies ran while one was open for 14% of the time, Pallas kernels for 0%

commit v1 on v0

v1 whole, which is shorter than its diff:
```python
import jax
import jax.numpy as jnp
from jax import lax
from jax.sharding import PartitionSpec as P

HD = 128


NORM_EPS = 1e-06
ROPE_BASE = 10000.0


def norm_rows(inputs, gain_vector):
    values = inputs.astype(jnp.float32)
    scaled = values * lax.rsqrt(jnp.mean(values * values, axis=-1, keepdims=True) + NORM_EPS)
    return (scaled * gain_vector).astype(jnp.bfloat16)


def rotate(head_rows, positions):
    head_size = head_rows.shape[-1]
    inverse = ROPE_BASE ** (-jnp.arange(0, head_size, 2, dtype=jnp.float32) / head_size)
    angles = positions[:, None] * inverse[None, :]
    cosine = jnp.cos(angles)[:, None, :]
    sine_part = jnp.sin(angles)[:, None, :]
    front_half = head_rows[..., : head_size // 2]
    behind = head_rows[..., head_size // 2 :]
    return jnp.concatenate(
        [front_half * cosine - behind * sine_part, front_half * sine_part + behind * cosine],
        axis=-1,
    )


def project(inputs, weight, head_total):
    product = jnp.dot(inputs, weight, preferred_element_type=jnp.float32).astype(jnp.bfloat16)
    product = lax.optimization_barrier(product)
    return product.astype(jnp.float32).reshape(inputs.shape[0], head_total, -1)


def retain_local(query_heads, key_heads, value_heads, decay_rates):
    length, head_total, head_size = query_heads.shape
    narrow = jnp.bfloat16
    log_gamma = -decay_rates
    place = lax.axis_index("ep")
    inner_pos = jnp.arange(length, dtype=jnp.float32)
    key_scale = jnp.exp(log_gamma[None, :] * (length - 1.0 - inner_pos)[:, None])
    summary = jnp.einsum(
        "nhd,nhe->hde",
        (key_heads * key_scale[:, :, None]).astype(narrow),
        value_heads.astype(narrow),
        preferred_element_type=jnp.float32,
    )
    gathered = lax.all_gather(summary, "ep")
    gaps = (place - 1 - jnp.arange(gathered.shape[0])).astype(jnp.float32)
    mix = jnp.where(
        gaps[:, None] >= 0,
        jnp.exp(log_gamma[None, :] * length * jnp.maximum(gaps, 0.0)[:, None]),
        0.0,
    )
    incoming = jnp.sum(mix[:, :, None, None] * gathered, axis=0)
    offsets = inner_pos[:, None] - inner_pos[None, :]
    decay_mask = jnp.where(
        offsets >= 0, jnp.exp(log_gamma[:, None, None] * jnp.maximum(offsets, 0.0)), 0.0
    )
    scores = (
        jnp.einsum(
            "nhd,mhd->hnm",
            query_heads.astype(narrow),
            key_heads.astype(narrow),
            preferred_element_type=jnp.float32,
        )
        * decay_mask
    )
    nearby = jnp.einsum(
        "hnm,mhe->nhe",
        scores.astype(narrow),
        value_heads.astype(narrow),
        preferred_element_type=jnp.float32,
    )
    query_scale = jnp.exp(log_gamma[None, :] * (inner_pos + 1.0)[:, None])
    distant = jnp.einsum(
        "nhd,hde->nhe",
        (query_heads * query_scale[:, :, None]).astype(narrow),
        incoming.astype(narrow),
        preferred_element_type=jnp.float32,
    )
    retained = nearby + distant
    normed = retained * lax.rsqrt(jnp.mean(retained * retained, axis=-1, keepdims=True) + NORM_EPS)
    return normed.astype(jnp.bfloat16).reshape(length, head_total * head_size)


def assign_slots(routes, source_rows, capacity, expert_count):
    token_count, pick_count = routes.shape
    chosen = routes.reshape(token_count * pick_count)
    onehot = (chosen[:, None] == jnp.arange(expert_count, dtype=jnp.int32)[None, :]).astype(
        jnp.int32
    )
    per_source = onehot.reshape(token_count // source_rows, source_rows * pick_count, expert_count)
    earlier_hits = jnp.cumsum(per_source, axis=1) - per_source
    ranks = jnp.sum(earlier_hits * per_source, axis=2).reshape(token_count * pick_count)
    sources = jnp.arange(token_count * pick_count, dtype=jnp.int32) // (source_rows * pick_count)
    return (chosen, sources * capacity + ranks)


def gather_slots(token_rows, chosen, slot_ids, slot_count, expert_count, pick_count):
    owners = jnp.arange(chosen.shape[0], dtype=jnp.int32) // pick_count + 1
    owner_table = jnp.zeros((slot_count, expert_count), jnp.int32).at[slot_ids, chosen].set(owners)
    padded = jnp.concatenate(
        [jnp.zeros((1, token_rows.shape[1]), token_rows.dtype), token_rows], axis=0
    )
    return padded[owner_table]


def expert_hidden(routed_rows, gate_weight, up_weight):
    per_device = gate_weight.shape[0]
    grouped = routed_rows.reshape(
        routed_rows.shape[0], routed_rows.shape[1] // per_device, per_device, routed_rows.shape[2]
    )
    gate_part = jnp.einsum(
        "snxd,xdf->snxf", grouped, gate_weight, preferred_element_type=jnp.float32
    )
    up_part = jnp.einsum("snxd,xdf->snxf", grouped, up_weight, preferred_element_type=jnp.float32)
    return (jax.nn.silu(gate_part) * up_part).astype(jnp.bfloat16)


def routed_dense(own_rows, routing, route_weight, gate_weight, up_weight, down_weight):
    own_count = own_rows.shape[0]
    local_experts = gate_weight.shape[0]
    expert_count = lax.axis_size("ep") * local_experts
    start = lax.axis_index("tp") * own_count
    own_routing = lax.dynamic_slice_in_dim(routing, start, own_count, 0)
    own_weight = lax.dynamic_slice_in_dim(route_weight, start, own_count, 0)
    named = own_routing[:, :, None] == jnp.arange(expert_count, dtype=jnp.int32)
    spread = jnp.sum(jnp.where(named, own_weight[:, :, None], 0.0), axis=1)
    rows = lax.all_gather(own_rows, "ep", axis=0, tiled=True)
    gate_all = lax.all_gather(gate_weight, "tp", axis=0)
    up_all = lax.all_gather(up_weight, "tp", axis=0)
    down_all = lax.all_gather(down_weight, "tp", axis=0)
    scales = lax.all_gather(spread, "ep", axis=0, tiled=True)
    scales = lax.dynamic_slice_in_dim(
        scales, lax.axis_index("ep") * local_experts, local_experts, 1
    )
    parts = gate_all.shape[0]
    total = None
    for x in range(local_experts):
        hidden = jnp.concatenate(
            [
                (
                    jax.nn.silu(jnp.dot(rows, gate_all[p, x], preferred_element_type=jnp.float32))
                    * jnp.dot(rows, up_all[p, x], preferred_element_type=jnp.float32)
                ).astype(jnp.bfloat16)
                for p in range(parts)
            ],
            axis=1,
        )
        result = jnp.concatenate(
            [
                jnp.dot(hidden, down_all[p, x], preferred_element_type=jnp.float32)
                * scales[:, x : x + 1]
                for p in range(parts)
            ],
            axis=1,
        )
        total = result if total is None else total + result
    summed = lax.psum_scatter(
        total.astype(jnp.bfloat16), "ep", scatter_dimension=0, tiled=True
    )
    return lax.all_to_all(summed, "tp", split_axis=1, concat_axis=0, tiled=True).astype(jnp.float32)


def routed_sparse(own_rows, routing, route_weight, gate_weight, up_weight, down_weight, capacity):
    own_count = own_rows.shape[0]
    tp_index = lax.axis_index("tp")
    group_count, pick_count = routing.shape
    expert_count = lax.axis_size("ep") * gate_weight.shape[0]
    chosen, slot_ids = assign_slots(routing, own_count, capacity, expert_count)
    own_span = own_count * pick_count
    own_chosen = lax.dynamic_slice_in_dim(chosen, tp_index * own_span, own_span, 0)
    own_slots = (
        lax.dynamic_slice_in_dim(slot_ids, tp_index * own_span, own_span, 0) - tp_index * capacity
    )
    outgoing = gather_slots(own_rows, own_chosen, own_slots, capacity, expert_count, pick_count)
    arrived = lax.all_to_all(outgoing, "ep", split_axis=1, concat_axis=1, tiled=True)
    hidden = expert_hidden(
        lax.all_gather(arrived, "tp", axis=0, tiled=True), gate_weight, up_weight
    )
    full_hidden = lax.all_gather(hidden, "tp", axis=3, tiled=True)
    results = jnp.einsum(
        "snxf,xfe->snxe", full_hidden, down_weight, preferred_element_type=jnp.float32
    ).astype(jnp.bfloat16)
    results = results.reshape(results.shape[0], expert_count, results.shape[3])
    returned = lax.all_to_all(results, "ep", split_axis=1, concat_axis=1, tiled=True)
    flat_results = returned.reshape(returned.shape[0] * expert_count, returned.shape[2])
    picked = flat_results[slot_ids * expert_count + chosen].astype(jnp.float32)
    return jnp.sum(picked.reshape(group_count, pick_count, -1) * route_weight[:, :, None], axis=1)


def shards(
    mixer_input,
    expert_input,
    mixer_gain,
    expert_gain,
    query_weight,
    key_weight,
    value_weight,
    out_weight,
    decay_rate,
    routing,
    route_weight,
    gate_weight,
    up_weight,
    down_weight,
    shared_gate,
    shared_up,
    shared_down,
):
    own_count = mixer_input.shape[0]
    own_expert_rows = norm_rows(expert_input, expert_gain)
    mixer_rows, expert_rows = (
        lax.all_gather(norm_rows(mixer_input, mixer_gain), "tp", axis=0, tiled=True),
        lax.all_gather(own_expert_rows, "tp", axis=0, tiled=True),
    )
    group_count = mixer_rows.shape[0]
    head_total = decay_rate.shape[0]
    positions = (
        lax.axis_index("ep") * group_count + jnp.arange(group_count, dtype=jnp.int32)
    ).astype(jnp.float32)
    query_heads = rotate(project(mixer_rows, query_weight, head_total), positions) * HD ** (-0.5)
    key_heads = rotate(project(mixer_rows, key_weight, head_total), positions)
    value_heads = project(mixer_rows, value_weight, head_total)
    mixed_heads = retain_local(query_heads, key_heads, value_heads, decay_rate)
    mixer_output = lax.psum_scatter(
        jnp.dot(mixed_heads, out_weight, preferred_element_type=jnp.float32).astype(jnp.bfloat16),
        "tp",
        scatter_dimension=0,
        tiled=True,
    ).astype(jnp.float32)
    expert_count = lax.axis_size("ep") * gate_weight.shape[0]
    pick_count = routing.shape[1]
    capacity = (3 * own_count * pick_count + 2 * expert_count - 1) // (2 * expert_count)
    experts = (own_expert_rows, routing, route_weight, gate_weight, up_weight, down_weight)
    if 2 * capacity >= own_count:
        weighted = routed_dense(*experts)
    else:
        weighted = routed_sparse(*experts, capacity)
    shared_hidden = (
        jax.nn.silu(jnp.dot(expert_rows, shared_gate, preferred_element_type=jnp.float32))
        * jnp.dot(expert_rows, shared_up, preferred_element_type=jnp.float32)
    ).astype(jnp.bfloat16)
    full_shared = lax.all_gather(shared_hidden, "tp", axis=1, tiled=True)
    shared_result = jnp.dot(full_shared, shared_down, preferred_element_type=jnp.float32)
    expert_output = weighted + shared_result
    return (mixer_output, expert_output)


def solution(mesh):
    return jax.shard_map(
        shards,
        mesh=mesh,
        in_specs=(
            P(("ep", "tp"), None),
            P(("ep", "tp"), None),
            P(),
            P(),
            P(None, "tp"),
            P(None, "tp"),
            P(None, "tp"),
            P("tp", None),
            P("tp"),
            P("ep", None),
            P("ep", None),
            P("ep", None, "tp"),
            P("ep", None, "tp"),
            P("ep", None, "tp"),
            P(None, "tp"),
            P(None, "tp"),
            P(None, "tp"),
        ),
        out_specs=(P(("ep", "tp"), None), P("ep", "tp")),
        check_vma=False,
    )
```

time: 452 us -> 419 us (0.927)
  waiting for transfers between devices: 196 us -> 275 us
  blocking collectives: 107 us -> 41 us
  local copies, waits for them, and re-layouts: 57.9 us -> 13.3 us
    unnamed x6 -> x10, waiting for transfers between devices: 0.62 us -> 92.2 us
    all_to_all x1 -> x0, blocking collectives: 77.9 us -> none  [shards(): lax.all_to_all(outgoing, 'ep', split_axis=1, concat_axis=1, tiled=True)]
    all_gather x1 -> x2, blocking collectives: 7.66 us -> 41 us  [the longest x1 30.8 us: routed_dense(): scales = lax.all_gather(spread, 'ep', axis=0, tiled=True)]
    scatter x1 -> x0, local copies, waits for them, and re-layouts: 22 us -> none  [gather_slots(): jnp.zeros((slot_count, expert_count), jnp.int32).at[slot_ids, chosen]]
    unnamed x1 -> x0, blocking collectives: 21.2 us -> none
    all_gather x3 -> x5, waiting for transfers between devices: 156 us -> 137 us  [the longest x1 67.1 us: routed_dense(): rows = lax.all_gather(own_rows, 'ep', axis=0, tiled=True)]
    gather x3 -> x0, local copies, waits for them, and re-layouts: 17.7 us -> none  [the longest x1 9.88 us: shards(): picked = flat_results[slot_ids * expert_count + chosen].astype(jnp.float32)]
    all_gather x1, waiting for transfers between devices: 6.17 us -> 18.2 us  [shards(): lax.all_gather(norm_rows(mixer_input, mixer_gain), 'tp', axis=0, tiled=True)]
  transfers between devices with their start and end apart: 7 -> 10, of which waited for: 6 -> 8; matrix products, arithmetic and copies ran while one was open for 14% -> 18% of each run, Pallas kernels for 0% -> 0%
where the time goes in v1:
time: 419 us; the launch traced here: 418 us
  waiting for transfers between devices  275 us (66%)
  matrix products  52.8 us (13%)
  blocking collectives  41 us (10%)
  other arithmetic  17.6 us (4%)
  between operations  14.1 us (3%)
  local copies, waits for them, and re-layouts  13.3 us (3%)
    unnamed x10, waiting for transfers between devices  92.2 us
    all_gather x1, waiting for transfers between devices, routed_dense(): rows = lax.all_gather(own_rows, 'ep', axis=0, tiled=True)  67.1 us
    all_gather x1, blocking collectives, routed_dense(): scales = lax.all_gather(spread, 'ep', axis=0, tiled=True)  30.8 us
    all_gather x1, waiting for transfers between devices, routed_dense(): up_all = lax.all_gather(up_weight, 'tp', axis=0)  24.7 us
    all_gather x1, waiting for transfers between devices, retain_local(): gathered = lax.all_gather(summary, 'ep')  23.8 us
    all_gather x1, waiting for transfers between devices, routed_dense(): down_all = lax.all_gather(down_weight, 'tp', axis=0)  21 us
    all_gather x1, waiting for transfers between devices, shards(): lax.all_gather(norm_rows(mixer_input, mixer_gain), 'tp', axis=0, tiled=True)  18.2 us
    reduce_scatter x1, waiting for transfers between devices, shards(): lax.psum_scatter(jnp.dot(mixed_heads, out_weight, preferred_element_type=...  15 us
  transfers between devices with their start and end apart: 10, of which 8 were waited for; matrix products, arithmetic and copies ran while one was open for 18% of the time, Pallas kernels for 0%

profile of v1, /device:TPU:0, one launch (start us, length us, event | category | flops | bytes accessed | tf_op | source)
XLA Modules:
  0.0 418.2 jit_solution(8707406454495204307)
XLA Ops:
  8.6 2.0 fusion.10
  12.7 2.1 fusion.13
  17.9 18.2 %all-gather.12.cloned.1.call-done = bf16[512,2048]{1,0:T(8,128)(2,1)} async-done(((bf16[128,2048]{1,0:T(8,128)(2,1)}), bf16[512,2048]{1,0:T(8,128)(2,1)}) %all-gather.12.cloned.1.call-update) | async-done | bytes 2097168 | tf_op jit(solution)/shard_map/all_gather | solution.py:219
  36.1 2.3 convolution_convert_fusion.2
  38.7 2.6 convolution_convert_fusion.1
  41.5 2.6 convolution_convert_fusion.3
  49.1 30.8 %all_gather.49 = f32[1024,8]{0,1:T(8,128)S(1)} all-gather(f32[128,8]{0,1:T(8,128)S(1)} %select_reduce_fusion), channel_id=1, replica_groups=mesh['ep'=8,'tp'=4] {'ep'}, dimensions={0}, use_global_device_ids=true | all-gather | bytes 36864 | tf_op jit(solution)/shard_map/all_gather | solution.py:138
  80.0 67.1 %all-gather.14.cloned.1.call-done = bf16[1024,2048]{1,0:T(8,128)(2,1)} async-done(((bf16[128,2048]{1,0:T(8,128)(2,1)}), bf16[1024,2048]{1,0:T(8,128)(2,1)}) %all-gather.14.cloned.1.call-update) | async-done | bytes 4194320 | tf_op jit(solution)/shard_map/all_gather | solution.py:134
  147.1 4.9 %fusion.17 = f32[1024,256]{0,1:T(8,128)} fusion(bf16[1024,2048]{1,0:T(8,128)(2,1)} %all-gather.14.cloned.1.call-done, bf16[4,2048,256]{2,1,0:T(8,128)(2,1)} %all-gather.20.cloned.1.call-done), kind=kOutput, calls=%fused_computation.50 | convolution fusion | flops 1073741824 | bytes 6291456 | tf_op jit(solution)/shard_map/dot_general | solution.py:148
  152.3 2.3 fusion.16
  154.6 2.3 fusion.15
  156.9 24.7 %all-gather.22.cloned.1.call-done = bf16[4,2048,256]{2,1,0:T(8,128)(2,1)} async-done(((bf16[1,2048,256]{2,1,0:T(8,128)(2,1)}), bf16[4,2048,256]{2,1,0:T(8,128)(2,1)}) %all-gather.22.cloned.1.call-update) | async-done | bytes 4194320 | tf_op jit(solution)/shard_map/all_gather | solution.py:136
  181.6 5.1 %fusion.1 = bf16[1024,256]{0,1:T(8,128)(2,1)} fusion(bf16[1024,2048]{1,0:T(8,128)(2,1)} %all-gather.14.cloned.1.call-done, bf16[4,2048,256]{2,1,0:T(8,128)(2,1)} %all-gather.22.cloned.1.call-done, f32[1024,256]{0,1:T(8,128)} %fusion.17), kind=kOutput, calls=%fused_computation.18 | convolution fusion | flops 1075314688 | bytes 6815744 | tf_op jit(solution)/shard_map/dot_general | solution.py:149
  187.3 2.2 fusion.2
  189.5 2.2 fusion.3
  191.6 2.6 fusion.14
  194.2 2.2 fusion.4
  196.4 21.0 %all-gather.24.cloned.1.call-done = bf16[4,1024,512]{2,1,0:T(8,128)(2,1)} async-done(((bf16[1,1024,512]{2,1,0:T(8,128)(2,1)}), bf16[4,1024,512]{2,1,0:T(8,128)(2,1)}) %all-gather.24.cloned.1.call-update) | async-done | bytes 4194320 | tf_op jit(solution)/shard_map/all_gather | solution.py:137
  217.5 3.3 multiply_convert_fusion
  225.3 2.4 pad_maximum_fusion
  227.8 6.6 %copy.61 = bf16[1024,2048]{1,0:T(8,128)(2,1)} copy(bf16[1024,2048]{0,1:T(8,128)(2,1)} %pad_maximum_fusion) | data formatting | bytes 8388608
  235.9 23.8 %all-gather.18.cloned.1.call-done = f32[16,128,128]{2,1,0:T(8,128)} async-done(((f32[2,128,128]{2,1,0:T(8,128)}), f32[16,128,128]{2,1,0:T(8,128)}) %all-gather.18.cloned.1.call-update) | async-done | bytes 1048592 | tf_op jit(solution)/shard_map/all_gather | solution.py:52
  262.4 3.4 multiply_reduce_fusion.1
  267.0 2.1 convolution_convert_fusion
  269.2 13.4 %all-gather.16.cloned.1.call-done = bf16[512,2048]{1,0:T(8,128)(2,1)} async-done(((bf16[128,2048]{1,0:T(8,128)(2,1)}), bf16[512,2048]{1,0:T(8,128)(2,1)}) %all-gather.16.cloned.1.call-update) | async-done | bytes 2097168 | tf_op jit(solution)/shard_map/all_gather | solution.py:220
  282.6 2.3 fusion.48
  284.9 89.7 %reduce-scatter.7.cloned.1.call-done = bf16[128,2048]{1,0:T(8,128)(2,1)} async-done(((bf16[1024,2048]{1,0:T(8,128)(2,1)}), bf16[128,2048]{1,0:T(8,128)(2,1)}) %reduce-scatter.7.cloned.1.call-update) | async-done | bytes 524304
  376.9 3.6 all-to-all-start
  380.5 2.3 fusion.7
  382.9 10.1 %all_gather.51 = bf16[512,512]{1,0:T(8,128)(2,1)S(1)} all-gather(bf16[512,128]{1,0:T(8,128)(2,1)S(1)} %fusion.7), channel_id=1, replica_groups=mesh['ep'=8,'tp'=4] {'tp'}, dimensions={1}, use_global_device_ids=true | all-gather | bytes 655360 | tf_op jit(solution)/shard_map/all_gather | solution.py:249
  393.0 15.0 %reduce-scatter.5.cloned.1.call-done = bf16[128,2048]{1,0:T(8,128)(2,1)} async-done(((bf16[512,2048]{1,0:T(8,128)(2,1)}), bf16[128,2048]{1,0:T(8,128)(2,1)}) %reduce-scatter.5.cloned.1.call-update) | async-done | bytes 524304 | tf_op jit(solution)/shard_map/reduce_scatter | solution.py:231
  408.0 2.1 convert_element_type.114
  (93 shorter events, 26.8 us)
Async XLA Ops:
  7.2 259.8 %copy-start = (bf16[256,2048]{1,0:T(8,128)(2,1)S(1)}, bf16[256,2048]{1,0:T(8,128)(2,1)}, u32[]{:S(2)}) copy-start(bf16[256,2048]{1,0:T(8,128)(2,1)} %param.24) | copy-start | bytes 3145732
  7.2 8.9 %copy-start.12 = (f32[2]{0:T(128)S(1)}, f32[2]{0:T(128)}, u32[]{:S(2)}) copy-start(f32[2]{0:T(128)} %param.25) | copy-start | bytes 28
  7.2 28.9 %copy-start.10 = (bf16[2048,256]{1,0:T(8,128)(2,1)S(1)}, bf16[2048,256]{1,0:T(8,128)(2,1)}, u32[]{:S(2)}) copy-start(bf16[2048,256]{1,0:T(8,128)(2,1)} %param.21) | copy-start | bytes 3145732
  7.2 28.9 %all-gather.12.cloned.1.call-start = ((), (), s32[]{:S(2)}) async-start(), calls=%async_computation.3 | async-start | bytes 2621440 | tf_op jit(solution)/shard_map/all_gather | solution.py:219
  10.7 69.3 %all-gather.20.cloned.1.call-start = ((), (), s32[]{:S(2)}) async-start(), calls=%async_computation.8 | async-start | bytes 5242880 | tf_op jit(solution)/shard_map/all_gather | solution.py:135
  11.4 135.7 %all-gather.14.cloned.1.call-start = ((), (), s32[]{:S(2)}) async-start(), calls=%async_computation.5 | async-start | bytes 4718592 | tf_op jit(solution)/shard_map/all_gather | solution.py:134
  14.8 166.8 %all-gather.22.cloned.1.call-start = ((), (), s32[]{:S(2)}) async-start(), calls=%async_computation.9 | async-start | bytes 5242880 | tf_op jit(solution)/shard_map/all_gather | solution.py:136
  15.4 202.1 %all-gather.24.cloned.1.call-start = ((), (), s32[]{:S(2)}) async-start(), calls=%async_computation.10 | async-start | bytes 5242880 | tf_op jit(solution)/shard_map/all_gather | solution.py:137
  16.0 243.8 %all-gather.18.cloned.1.call-start = ((), (), s32[]{:S(2)}) async-start(), calls=%async_computation.7 | async-start | bytes 1179648 | tf_op jit(solution)/shard_map/all_gather | solution.py:52
  41.5 3.8 copy-start.1
  44.1 1.4 copy-start.4
  46.9 235.7 %all-gather.16.cloned.1.call-start = ((), (), s32[]{:S(2)}) async-start(), calls=%async_computation.6 | async-start | bytes 2621440 | tf_op jit(solution)/shard_map/all_gather | solution.py:220
  47.7 326.9 %reduce-scatter.7.cloned.1.call-start = ((), (), s32[]{:S(2)}) async-start(), calls=%async_computation.11 | async-start | bytes 4718592
  147.1 4.9 %copy-start.5 = (bf16[4,2048,256]{2,1,0:T(8,128)(2,1)S(1)}, bf16[4,2048,256]{2,1,0:T(8,128)(2,1)}, u32[]{:S(2)}) copy-start(bf16[4,2048,256]{2,1,0:T(8,128)(2,1)} %all-gather.20.cloned.1.call-done) | copy-start | bytes 12582916
  147.1 5.2 %copy-start.6 = (bf16[1024,2048]{1,0:T(8,128)(2,1)S(1)}, bf16[1024,2048]{1,0:T(8,128)(2,1)}, u32[]{:S(2)}) copy-start(bf16[1024,2048]{1,0:T(8,128)(2,1)} %all-gather.14.cloned.1.call-done) | copy-start | bytes 12582916
  181.6 5.1 %copy-start.7 = (bf16[1024,2048]{1,0:T(8,128)(2,1)S(1)}, bf16[1024,2048]{1,0:T(8,128)(2,1)}, u32[]{:S(2)}) copy-start(bf16[1024,2048]{1,0:T(8,128)(2,1)} %all-gather.14.cloned.1.call-done) | copy-start | bytes 12582916
  181.6 5.3 %copy-start.9 = (bf16[4,2048,256]{2,1,0:T(8,128)(2,1)S(1)}, bf16[4,2048,256]{2,1,0:T(8,128)(2,1)}, u32[]{:S(2)}) copy-start(bf16[4,2048,256]{2,1,0:T(8,128)(2,1)} %all-gather.22.cloned.1.call-done) | copy-start | bytes 12582916
  181.6 5.7 %copy-start.14 = (f32[1024,256]{0,1:T(8,128)S(1)}, f32[1024,256]{0,1:T(8,128)}, u32[]{:S(2)}) copy-start(f32[1024,256]{0,1:T(8,128)} %fusion.16) | copy-start | bytes 3145732
  187.3 2.2 copy-start.13
  217.5 3.3 copy-start.8
  217.5 3.3 copy-start.15
  217.5 3.4 copy-start.16
  217.5 3.6 copy-start.17
  217.5 3.7 copy-start.18
  234.4 173.6 %reduce-scatter.5.cloned.1.call-start = ((), (), s32[]{:S(2)}) async-start(), calls=%async_computation.4 | async-start | bytes 2621440 | tf_op jit(solution)/shard_map/reduce_scatter | solution.py:231
  265.8 16.8 %copy-start.2 = (bf16[2048,128]{1,0:T(8,128)(2,1)S(1)}, bf16[2048,128]{1,0:T(8,128)(2,1)}, u32[]{:S(2)}) copy-start(bf16[2048,128]{1,0:T(8,128)(2,1)} %param.31) | copy-start | bytes 1572868
  269.1 111.4 %copy-start.11 = (bf16[2048,128]{1,0:T(8,128)(2,1)S(1)}, bf16[2048,128]{1,0:T(8,128)(2,1)}, u32[]{:S(2)}) copy-start(bf16[2048,128]{1,0:T(8,128)(2,1)} %param.32) | copy-start | bytes 1572868
  376.9 33.3 %copy-start.3 = (bf16[512,512]{1,0:T(8,128)(2,1)S(1)}, bf16[512,512]{1,0:T(8,128)(2,1)}, u32[]{:S(2)}) copy-start(bf16[512,512]{1,0:T(8,128)(2,1)} %param.33) | copy-start | bytes 1572868
  376.9 33.2 %all-to-all-start = ((bf16[128,4,512]{2,0,1:T(8,128)(2,1)}), bf16[128,4,512]{2,0,1:T(8,128)(2,1)S(1)}, u32[]{:S(2)}, u32[]{:S(2)}) async-start(bf16[128,4,512]{2,0,1:T(8,128)(2,1)} %copy.58), calls=%async_computation.1 | async-start | bytes 1048576 | tf_op jit(solution)/shard_map/all_to_all | solution.py:167
Sparse Core Ops, SparseCore 0:
  10.8 25.2 all-gather.11
  37.7 34.4 all-gather.19
  74.3 72.7 all-gather.13
  148.5 32.9 all-gather.21
  183.0 34.4 all-gather.23
  219.4 40.2 all-gather.17
  261.3 21.2 all-gather.15
  286.2 88.2 reduce-scatter.6
  377.1 30.8 reduce-scatter.4
